TPU v7x, 32 devices: a whole 2x2x4 slice. The times are simulated.
32 devices in a mesh: sp: 4 (over y, x), tp: 8 (over z, core).
Axes of the slice: x: 2, y: 2, z: 4, core: 2. Of those that a mesh axis runs over, the one named last changes fastest.
Arguments:
- query_rows: bfloat16 [8192, 1024], P('sp', 'tp'), may hold values from -6 to 6
- key_rows: bfloat16 [8192, 1024], P('sp', 'tp'), may hold values from -6 to 6
- value_rows: bfloat16 [8192, 1024], P('sp', 'tp'), may hold values from -6 to 6
- gate_rows: bfloat16 [8192, 1024], P('sp', 'tp'), may hold values from -6 to 6
- log_decay: float32 [16, 8192], P('tp', 'sp'), may hold values from -1 to 0
- residual: bfloat16 [8192, 2048], P(('sp', 'tp')), may hold values from -6 to 6
- head_gain: float32 [1024], P('tp'), may hold values from 0.1 to 1.9
- out_weight: bfloat16 [1024, 2048], P(None, 'tp'), may hold values from -0.1875 to 0.1875
- norm_gain: float32 [2048], replicated, may hold values from 0.1 to 1.9
- expert_ids: int32 [8192, 2], P(('sp', 'tp')), may hold values from 0 to 3, all different within a row; in each aligned block of 256 rows (0 to 255, 256 to 511, ...) at most 192 rows name the same one
- route_weights: float32 [8192, 2], P(('sp', 'tp')), may hold values from 0.2 to 1
- expert_gate: bfloat16 [2048, 4096], P(None, ('sp', 'tp')), may hold values from -0.125 to 0.125
- expert_up: bfloat16 [2048, 4096], P(None, ('sp', 'tp')), may hold values from -0.125 to 0.125
- expert_down: bfloat16 [2048, 4096], P(None, ('sp', 'tp')), may hold values from -0.1875 to 0.1875
- shared_gate: bfloat16 [2048, 512], replicated, may hold values from -0.125 to 0.125
- shared_up: bfloat16 [2048, 512], replicated, may hold values from -0.125 to 0.125
- shared_down: bfloat16 [2048, 512], replicated, may hold values from -0.25 to 0.25
Outputs:
- result: bfloat16 [8192, 2048], P(('sp', 'tp'))
Inputs may be any that keep to these rules, and one draw needn't show every extreme that they name: `expert_ids`: each row names 2 different experts. Within the rows of one device (aligned blocks of 256 rows) no expert is named by more than 192 rows, and in some block an expert is named by exactly 192 rows.
All inputs are finite; a program needn't handle non-finite values.
Results may differ from a plain program's by a relative error of at most 0.0075.
Values may be sent and summed in bfloat16 or wider, within the bound.
A program may use at most 128 MiB of HBM per device.

v0:
```python
import jax
import jax.numpy as jnp
from jax import lax
from jax.sharding import PartitionSpec as P

HEAD = 64
SPAN = 512


eps = 1e-05


def entering(value, axis, join, neutral):
    count, mine = (lax.axis_size(axis), lax.axis_index(axis))
    pieces = jax.tree.map(lambda part: lax.all_gather(part, axis), value)
    so_far = jax.tree.map(
        lambda part, zero: jnp.full_like(part, 0) + jnp.asarray(zero, part.dtype), value, neutral
    )

    def hop(position, so_far):
        longer = join(so_far, jax.tree.map(lambda part: part[position], pieces))
        return jax.tree.map(lambda new, old: jnp.where(position < mine, new, old), longer, so_far)

    return lax.fori_loop(0, count - 1, hop, so_far)


def block_pass(queries, key_heads, values, log_decay, state):
    rows, heads, width = queries.shape
    count = rows // SPAN
    scale = width ** (-0.5)
    query_blocks = queries.reshape(count, SPAN, heads, width)
    key_blocks = key_heads.reshape(count, SPAN, heads, width)
    value_blocks = values.reshape(count, SPAN, heads, width)
    decay_blocks = log_decay.reshape(heads, count, SPAN).transpose(1, 0, 2)
    offsets = jnp.arange(SPAN, dtype=jnp.int32)
    causal = offsets[:, None] >= offsets[None, :]

    def advance(carry, inputs):
        block_queries, block_keys, block_values, decay_block = inputs
        running = jnp.cumsum(decay_block, axis=1)
        spread = running[:, :, None] - running[:, None, :]
        damping = jnp.exp(jnp.where(causal[None], spread, -jnp.inf))
        attention_scores = jnp.einsum(
            "xru,jru->rxj", block_queries, block_keys, preferred_element_type=jnp.float32
        )
        decay_weighted = (attention_scores * scale * damping).astype(jnp.bfloat16)
        inner_block_term = jnp.einsum(
            "svc,csj->vsj", decay_weighted, block_values, preferred_element_type=jnp.float32
        )
        carried = jnp.einsum(
            "nhd,hde->nhe",
            block_queries.astype(jnp.float32),
            carry,
            precision=lax.Precision.HIGHEST,
        )
        carried = carried * jnp.exp(running).T[:, :, None]
        decay_to_block_end = jnp.exp(running[:, -1:] - running).T[:, :, None] * scale
        state_update = jnp.einsum(
            "jok,jow->okw",
            block_keys.astype(jnp.float32) * decay_to_block_end,
            block_values.astype(jnp.float32),
            precision=lax.Precision.HIGHEST,
        )
        carry = carry * jnp.exp(running[:, -1])[:, None, None] + state_update
        return (carry, inner_block_term + carried)

    final, outputs = lax.scan(
        advance, state, (query_blocks, key_blocks, value_blocks, decay_blocks)
    )
    return (final, outputs.reshape(rows, heads, width))


def combine_states(earlier, later):
    return (earlier[0] * later[0], earlier[1] * later[0][:, None, None] + later[1])


def entering_state(totals, own_state):
    identity = (jnp.ones_like(totals), jnp.zeros_like(own_state))
    return entering((totals, own_state), "sp", combine_states, identity)[1]


def on_device(
    query_rows,
    key_rows,
    value_rows,
    gate_rows,
    log_decay,
    residual,
    head_gain,
    out_weight,
    norm_gain,
    expert_ids,
    route_weights,
    expert_gate,
    expert_up,
    expert_down,
    shared_gate,
    shared_up,
    shared_down,
):
    seq_rows, local_width = query_rows.shape
    heads = local_width // HEAD
    out_full, gate_full, up_full, down_full = (
        lax.all_gather(out_weight, "tp", axis=1, tiled=True),
        lax.all_gather(expert_gate, "tp", axis=1, tiled=True),
        lax.all_gather(expert_up, "tp", axis=1, tiled=True),
        lax.all_gather(expert_down, "tp", axis=1, tiled=True),
    )
    queries = query_rows.reshape(seq_rows, heads, HEAD)
    key_heads = key_rows.reshape(seq_rows, heads, HEAD)
    values = value_rows.reshape(seq_rows, heads, HEAD)
    zero_state = jnp.zeros((heads, HEAD, HEAD), jnp.float32)
    running = jnp.cumsum(log_decay, axis=1)
    totals = jnp.exp(running[:, -1])
    own_state, retained = block_pass(queries, key_heads, values, log_decay, zero_state)
    incoming = entering_state(totals, own_state)
    readout = jnp.einsum(
        "nhd,hde->nhe", queries.astype(jnp.float32), incoming, precision=lax.Precision.HIGHEST
    )
    retained = retained + readout * jnp.exp(running).T[:, :, None]
    centered = retained - jnp.mean(retained, axis=2, keepdims=True)
    normed = centered * lax.rsqrt(jnp.mean(centered * centered, axis=2, keepdims=True) + eps)
    ret_rows = (
        normed.reshape(seq_rows, local_width)
        * head_gain
        * jax.nn.silu(gate_rows.astype(jnp.float32))
    ).astype(jnp.bfloat16)
    token_rows = lax.all_to_all(ret_rows, "tp", split_axis=0, concat_axis=1, tiled=True)
    mixer = jnp.dot(token_rows, out_full, preferred_element_type=jnp.float32)
    hidden = (residual.astype(jnp.float32) + mixer).astype(jnp.bfloat16)
    hidden_wide = hidden.astype(jnp.float32)
    normed_rows = (
        hidden_wide
        * lax.rsqrt(jnp.mean(hidden_wide * hidden_wide, axis=1, keepdims=True) + eps)
        * norm_gain
    ).astype(jnp.bfloat16)
    shared_mid = (
        jax.nn.silu(jnp.dot(normed_rows, shared_gate, preferred_element_type=jnp.float32))
        * jnp.dot(normed_rows, shared_up, preferred_element_type=jnp.float32)
    ).astype(jnp.bfloat16)
    shared_out = lax.dot_general(
        shared_mid, shared_down, (((1,), (1,)), ((), ())), preferred_element_type=jnp.float32
    )
    specialist_networks = lax.axis_size("sp")
    token_count, chosen_count = expert_ids.shape
    model_width = normed_rows.shape[1]
    capacity = 3 * token_count * chosen_count // (2 * specialist_networks)
    flat_ids = expert_ids.reshape(-1)
    matches = (
        flat_ids[:, None] == jnp.arange(specialist_networks, dtype=jnp.int32)[None, :]
    ).astype(jnp.int32)
    position = jnp.sum((jnp.cumsum(matches, axis=0) - 1) * matches, axis=1)
    slot = flat_ids * capacity + position
    owner = jnp.arange(token_count * chosen_count, dtype=jnp.int32) // chosen_count
    slot_token = jnp.zeros((specialist_networks * capacity,), jnp.int32).at[slot].set(owner)
    slot_live = jnp.zeros((specialist_networks * capacity,), jnp.bfloat16).at[slot].set(1.0)
    outgoing = (normed_rows[slot_token] * slot_live[:, None]).reshape(
        specialist_networks, capacity, model_width
    )
    arrived = lax.all_to_all(outgoing, "sp", split_axis=0, concat_axis=0, tiled=True)
    flat_rows = arrived.reshape(-1, model_width)
    middle = (
        jax.nn.silu(jnp.dot(flat_rows, gate_full, preferred_element_type=jnp.float32))
        * jnp.dot(flat_rows, up_full, preferred_element_type=jnp.float32)
    ).astype(jnp.bfloat16)
    outcome = lax.dot_general(
        middle, down_full, (((1,), (1,)), ((), ())), preferred_element_type=jnp.float32
    ).astype(jnp.bfloat16)
    processed = outcome.reshape(arrived.shape)
    returned = lax.all_to_all(processed, "sp", split_axis=0, concat_axis=0, tiled=True)
    picked = returned.reshape(specialist_networks * capacity, model_width)[slot].astype(jnp.float32)
    decay_weighted = picked * route_weights.reshape(-1)[:, None]
    routed = jnp.sum(decay_weighted.reshape(token_count, chosen_count, model_width), axis=1)
    return (hidden_wide + routed + shared_out).astype(jnp.bfloat16)


def solution(mesh):
    placed = (
        P("sp", "tp"),
        P("sp", "tp"),
        P("sp", "tp"),
        P("sp", "tp"),
        P("tp", "sp"),
        P(("sp", "tp"), None),
        P("tp"),
        P(None, "tp"),
        P(),
        P(("sp", "tp"), None),
        P(("sp", "tp"), None),
        P(None, ("sp", "tp")),
        P(None, ("sp", "tp")),
        P(None, ("sp", "tp")),
        P(),
        P(),
        P(),
    )
    return jax.shard_map(
        on_device, mesh=mesh, in_specs=placed, out_specs=P(("sp", "tp"), None), check_vma=False
    )
```

profile of v0, /device:TPU:0, one launch (start us, length us, event | category | flops | bytes accessed | tf_op | source)
XLA Modules:
  0.0 303.6 jit_solution(6103581982348177756)
XLA Ops:
  17.1 11.4 %all-reduce = f32[8]{0:T(128)S(1)} all-reduce(f32[8]{0:T(128)S(1)} %bitcast_dynamic-update-slice_fusion), channel_id=2, replica_groups=mesh['sp'=4,'tp'=8] {'sp'}, use_global_device_ids=true, to_apply=%add | all-reduce | flops 8 | bytes 64
  44.3 50.0 %while.27 = (s32[]{:T(128)}, f32[2,64,64]{2,1,0:T(8,128)S(1)}, f32[4,512,2,64]{1,0,3,2:T(4,128)}, f32[4,2,512]{2,1,0:T(2,128)S(1)}, bf16[4,512,2,64]{1,3,2,0:T(8...) while((s32[]{:T(128)}, f32[2,64,64]{2,1,0:T(8,128)S(1)}, ...), condition=%wide.region_3.4_spmd.clone, body=%wide.region_0.3_spmd.clone.sunk | while | flops 238192672 | bytes 3317096 | solution.py:67
  49.3 6.2 %dynamic_update_slice.6 = f32[4,512,2,64]{1,0,3,2:T(4,128)} dynamic-update-slice(f32[4,512,2,64]{1,0,3,2:T(4,128)} %get-tuple-element.330, f32[1,512,2,64]{1,0,3,2:T(1,128)S(1)} %copy.122, s32[]{:T(128)} %get-tuple-element.328, s32[]{:T(128)} %constant.94.clone.1..sunk, s32[]{:T(128)} %constant.94.clone.1..sunk, s32[]{:T(128)} %constant.94.clone.1..sunk) | dynamic-update-slice | bytes 524292 | tf_op jit(solution)/shard_map/while/body/jit(dynamic_update_index_in_dim)/dynamic_update_slice | solution.py:67
  61.9 6.2 %dynamic_update_slice.6 = f32[4,512,2,64]{1,0,3,2:T(4,128)} dynamic-update-slice(f32[4,512,2,64]{1,0,3,2:T(4,128)} %get-tuple-element.330, f32[1,512,2,64]{1,0,3,2:T(1,128)S(1)} %copy.122, s32[]{:T(128)} %get-tuple-element.328, s32[]{:T(128)} %constant.94.clone.1..sunk, s32[]{:T(128)} %constant.94.clone.1..sunk, s32[]{:T(128)} %constant.94.clone.1..sunk) | dynamic-update-slice | bytes 524292 | tf_op jit(solution)/shard_map/while/body/jit(dynamic_update_index_in_dim)/dynamic_update_slice | solution.py:67
  74.4 6.1 %dynamic_update_slice.6 = f32[4,512,2,64]{1,0,3,2:T(4,128)} dynamic-update-slice(f32[4,512,2,64]{1,0,3,2:T(4,128)} %get-tuple-element.330, f32[1,512,2,64]{1,0,3,2:T(1,128)S(1)} %copy.122, s32[]{:T(128)} %get-tuple-element.328, s32[]{:T(128)} %constant.94.clone.1..sunk, s32[]{:T(128)} %constant.94.clone.1..sunk, s32[]{:T(128)} %constant.94.clone.1..sunk) | dynamic-update-slice | bytes 524292 | tf_op jit(solution)/shard_map/while/body/jit(dynamic_update_index_in_dim)/dynamic_update_slice | solution.py:67
  86.9 6.1 %dynamic_update_slice.6 = f32[4,512,2,64]{1,0,3,2:T(4,128)} dynamic-update-slice(f32[4,512,2,64]{1,0,3,2:T(4,128)} %get-tuple-element.330, f32[1,512,2,64]{1,0,3,2:T(1,128)S(1)} %copy.122, s32[]{:T(128)} %get-tuple-element.328, s32[]{:T(128)} %constant.94.clone.1..sunk, s32[]{:T(128)} %constant.94.clone.1..sunk, s32[]{:T(128)} %constant.94.clone.1..sunk) | dynamic-update-slice | bytes 524292 | tf_op jit(solution)/shard_map/while/body/jit(dynamic_update_index_in_dim)/dynamic_update_slice | solution.py:67
  94.3 8.0 %all-gather.1 = f32[8,64,64]{2,1,0:T(8,128)S(1)} all-gather(f32[2,64,64]{2,1,0:T(8,128)S(1)} %get-tuple-element.143), channel_id=3, replica_groups=mesh['sp'=4,'tp'=8] {'sp'}, dimensions={0}, use_global_device_ids=true | all-gather | bytes 163840 | tf_op jit(solution)/shard_map/all_gather | solution.py:15
  113.3 4.8 %all-to-all-start = ((bf16[8,256,128]{2,1,0:T(8,128)(2,1)}), bf16[8,256,128]{2,1,0:T(8,128)(2,1)S(1)}, u32[]{:S(2)}, u32[]{:S(2)}) async-start(bf16[8,256,128]{2,1,0:T(8,128)(2,1)} %bitcast.159), calls=%async_computation | async-start | bytes 1048576 | tf_op jit(solution)/shard_map/all_to_all | solution.py:128
  123.1 3.8 %scatter_custom_fusion.1 = bf16[768]{0:T(1024)(128)(2,1)S(1)} fusion(s32[512]{0:T(512)S(1)} %bitcast.173, bf16[512]{0:T(512)(128)(2,1)S(1)} %broadcast.147, bf16[]{:T(256)} %constant.106.clone.1), kind=kCustom, calls=%fused_computation.116 | custom fusion | bytes 1538 | tf_op jit(solution)/shard_map/scatter | solution.py:156
  127.0 20.6 %all-to-all-done = bf16[8,256,128]{2,1,0:T(8,128)(2,1)S(1)} async-done(((bf16[8,256,128]{2,1,0:T(8,128)(2,1)}), bf16[8,256,128]{2,1,0:T(8,128)(2,1)S(1)}, u32[]{:S(2)}, u32[]{:S(2)}) %all-to-all-start) | async-done | bytes 524320 | tf_op jit(solution)/shard_map/all_to_all | solution.py:128
  147.9 4.0 %fusion.46 = (f32[256]{0:T(256)S(1)}, bf16[256,2048]{1,0:T(8,128)(2,1)S(1)}) fusion(bf16[256,1024]{0,1:T(8,128)(2,1)S(1)} %bitcast.163, bf16[1024,2048]{1,0:T(8,128)(2,1)} %all-gather.7.cloned.1.call-done, bf16[256,2048]{1,0:T(8,128)(2,1)} %param.26), kind=kOutput, calls=%fused_computation.66 | convolution fusion | flops 1076887296 | bytes 6816768 | tf_op jit(solution)/shard_map/dot_general | solution.py:129
  153.2 4.3 %gather_fusion = bf16[768,2048]{1,0:T(8,128)(2,1)} fusion(bf16[256,2048]{1,0:T(8,128)(2,1)S(1)} %fusion.48, s32[1024]{0:T(1024)S(1)} %pad_clamp_fusion.1), kind=kCustom, calls=%fused_computation | custom fusion | bytes 6294528 | tf_op jit(solution)/shard_map/gather | solution.py:157
  157.5 3.8 %broadcast_multiply_fusion = bf16[4,192,2048]{2,1,0:T(8,128)(2,1)} fusion(bf16[4,192,2048]{2,1,0:T(8,128)(2,1)} %bitcast.156, bf16[4,192]{1,0:T(4,128)(2,1)S(1)} %mul.185), kind=kLoop, calls=%fused_computation.69 | loop fusion | flops 1572864 | bytes 6292992 | tf_op jit(solution)/shard_map/mul | solution.py:157
  161.3 4.7 %all-to-all-start.1 = ((bf16[4,192,2048]{2,1,0:T(8,128)(2,1)}), bf16[4,192,2048]{2,1,0:T(8,128)(2,1)}, u32[]{:S(2)}, u32[]{:S(2)}) async-start(bf16[4,192,2048]{2,1,0:T(8,128)(2,1)} %broadcast_multiply_fusion), calls=%async_computation.1 | async-start | bytes 6291456 | tf_op jit(solution)/shard_map/all_to_all | solution.py:160
  166.1 36.7 %all-to-all-done.1 = bf16[4,192,2048]{2,1,0:T(8,128)(2,1)} async-done(((bf16[4,192,2048]{2,1,0:T(8,128)(2,1)}), bf16[4,192,2048]{2,1,0:T(8,128)(2,1)}, u32[]{:S(2)}, u32[]{:S(2)}) %all-to-all-start.1) | async-done | bytes 3145760 | tf_op jit(solution)/shard_map/all_to_all | solution.py:160
  202.7 8.3 %fusion.78 = f32[768,1024]{1,0:T(8,128)} fusion(bf16[768,2048]{1,0:T(8,128)(2,1)} %bitcast.16, bf16[2048,1024]{1,0:T(8,128)(2,1)} %all-gather.9.cloned.1.call-done), kind=kOutput, calls=%fused_computation.125 | convolution fusion | flops 3221225472 | bytes 10485760 | tf_op jit(solution)/shard_map/dot_general | solution.py:163
  211.0 3.9 %all-gather.13.cloned.1.call-done = bf16[2048,1024]{1,0:T(8,128)(2,1)} async-done(((bf16[2048,128]{1,0:T(8,128)(2,1)}), bf16[2048,1024]{1,0:T(8,128)(2,1)}) %all-gather.13.cloned.1.call-update) | async-done | bytes 4194320 | tf_op jit(solution)/shard_map/all_gather | solution.py:107
  214.9 12.5 %convolution_convert_fusion = bf16[768,2048]{1,0:T(8,128)(2,1)} fusion(bf16[2048,1024]{1,0:T(8,128)(2,1)} %all-gather.13.cloned.1.call-done, f32[768,1024]{1,0:T(8,128)} %fusion.78, bf16[768,2048]{1,0:T(8,128)(2,1)} %bitcast.16, bf16[2048,1024]{1,0:T(8,128)(2,1)} %all-gather.11.cloned.1.call-done), kind=kOutput, calls=%fused_computation.54 | convolution fusion | flops 6448742400 | bytes 17825792 | tf_op jit(solution)/shard_map/dot_general | solution.py:166
  227.5 5.0 %all-to-all-start.2 = ((bf16[4,192,2048]{2,1,0:T(8,128)(2,1)}), bf16[4,192,2048]{2,1,0:T(8,128)(2,1)}, u32[]{:S(2)}, u32[]{:S(2)}) async-start(bf16[4,192,2048]{2,1,0:T(8,128)(2,1)} %bitcast.158), calls=%async_computation.2 | async-start | bytes 6291456 | tf_op jit(solution)/shard_map/all_to_all | solution.py:170
  235.8 33.3 %all-to-all-done.2 = bf16[4,192,2048]{2,1,0:T(8,128)(2,1)} async-done(((bf16[4,192,2048]{2,1,0:T(8,128)(2,1)}), bf16[4,192,2048]{2,1,0:T(8,128)(2,1)}, u32[]{:S(2)}, u32[]{:S(2)}) %all-to-all-start.2) | async-done | bytes 3145760 | tf_op jit(solution)/shard_map/all_to_all | solution.py:170
  269.1 7.6 %gather_fusion.1 = bf16[512,2048]{1,0:T(8,128)(2,1)} fusion(bf16[768,2048]{1,0:T(8,128)(2,1)} %bitcast.18, s32[1024]{0:T(1024)S(1)} %pad_clamp_fusion), kind=kCustom, calls=%fused_computation.1 | custom fusion | bytes 4196352 | tf_op jit(solution)/shard_map/gather | solution.py:171
  276.7 5.4 %reshape.189 = f32[256,2,2048]{2,1,0:T(2,128)} reshape(bf16[512,2048]{1,0:T(8,128)(2,1)} %gather_fusion.1) | data formatting | bytes 6291456 | tf_op jit(solution)/shard_map/convert_element_type | solution.py:171
  282.1 10.1 %multiply_reduce_fusion = f32[256,2048]{1,0:T(8,128)} fusion(f32[256,2,2048]{2,1,0:T(2,128)} %reshape.189, f32[256,2]{1,0:T(8,128)S(1)} %copy.78), kind=kLoop, calls=%fused_computation.53 | loop fusion | flops 1572864 | bytes 6293504 | tf_op jit(solution)/shard_map/reduce_sum | solution.py:173
  292.3 4.8 %fusion.42 = bf16[256,2048]{1,0:T(8,128)(2,1)} fusion(bf16[2048,512]{1,0:T(8,128)(2,1)S(1)} %copy-done, f32[256,2048]{1,0:T(8,128)} %multiply_reduce_fusion, bf16[256,2048]{1,0:T(8,128)(2,1)S(1)} %copy-done.2, bf16[2048,512]{1,0:T(8,128)(2,1)} %param.36, f32[256,512]{1,0:T(8,128)} %fusion.76, f32[2048]{0:T(1024)S(1)} %copy-done.5, f32[256]{0:T(256)S(1)} %add_rsqrt_fusion.1), kind=kOutput, calls=%fused_computation.61 | convolution fusion | flops 1078722560 | bytes 8922112 | tf_op jit(solution)/shard_map/dot_general | solution.py:141
  (158 shorter events, 73.7 us)
Async XLA Ops:
  6.5 285.7 %copy-start = (bf16[2048,512]{1,0:T(8,128)(2,1)S(1)}, bf16[2048,512]{1,0:T(8,128)(2,1)}, u32[]{:S(2)}) copy-start(bf16[2048,512]{1,0:T(8,128)(2,1)} %param.37) | copy-start | bytes 6291460
  6.5 7.1 %copy-start.9 = (u32[32]{0:T(128)S(1)}, u32[32]{0:T(128)}, u32[]{:S(2)}) copy-start(u32[32]{0:T(128)} %constant.111) | copy-start | bytes 388
  6.5 2.8 copy-start.3
  6.5 141.3 %all-gather.7.cloned.1.call-start = ((), (), s32[]{:S(2)}) async-start(), calls=%async_computation.3 | async-start | bytes 4718592 | tf_op jit(solution)/shard_map/all_gather | solution.py:104
  7.3 158.8 %all-gather.9.cloned.1.call-start = ((), (), s32[]{:S(2)}) async-start(), calls=%async_computation.4 | async-start | bytes 4718592 | tf_op jit(solution)/shard_map/all_gather | solution.py:105
  8.0 203.0 %all-gather.11.cloned.1.call-start = ((), (), s32[]{:S(2)}) async-start(), calls=%async_computation.5 | async-start | bytes 4718592 | tf_op jit(solution)/shard_map/all_gather | solution.py:106
  8.7 206.2 %all-gather.13.cloned.1.call-start = ((), (), s32[]{:S(2)}) async-start(), calls=%async_computation.6 | async-start | bytes 4718592 | tf_op jit(solution)/shard_map/all_gather | solution.py:107
  94.3 12.3 %copy-start.4 = (f32[2048,2]{0,1:T(2,128)S(1)}, f32[2048,2]{0,1:T(2,128)}, u32[]{:S(2)}) copy-start(f32[2048,2]{0,1:T(2,128)} %exponential_bitcast_fusion.1) | copy-start | bytes 49156
  108.5 2.7 copy-start.8
  111.2 7.0 %copy-start.6 = (s32[256,2]{0,1:T(2,128)S(1)}, s32[256,2]{0,1:T(2,128)}, u32[]{:S(2)}) copy-start(s32[256,2]{0,1:T(2,128)} %param.30) | copy-start | bytes 6148
  113.3 34.3 %all-to-all-start = ((bf16[8,256,128]{2,1,0:T(8,128)(2,1)}), bf16[8,256,128]{2,1,0:T(8,128)(2,1)S(1)}, u32[]{:S(2)}, u32[]{:S(2)}) async-start(bf16[8,256,128]{2,1,0:T(8,128)(2,1)} %bitcast.159), calls=%async_computation | async-start | bytes 1048576 | tf_op jit(solution)/shard_map/all_to_all | solution.py:128
  147.9 5.0 %copy-start.5 = (f32[2048]{0:T(1024)S(1)}, f32[2048]{0:T(1024)}, u32[]{:S(2)}) copy-start(f32[2048]{0:T(1024)} %param.29) | copy-start | bytes 24580
  151.9 1.0 copy-start.1
  161.3 41.4 %all-to-all-start.1 = ((bf16[4,192,2048]{2,1,0:T(8,128)(2,1)}), bf16[4,192,2048]{2,1,0:T(8,128)(2,1)}, u32[]{:S(2)}, u32[]{:S(2)}) async-start(bf16[4,192,2048]{2,1,0:T(8,128)(2,1)} %broadcast_multiply_fusion), calls=%async_computation.1 | async-start | bytes 6291456 | tf_op jit(solution)/shard_map/all_to_all | solution.py:160
  227.5 5.0 %copy-start.7 = (f32[256,2]{0,1:T(2,128)S(1)}, f32[256,2]{0,1:T(2,128)}, u32[]{:S(2)}) copy-start(f32[256,2]{0,1:T(2,128)} %param.31) | copy-start | bytes 6148
  227.5 5.2 %copy-start.2 = (bf16[256,2048]{1,0:T(8,128)(2,1)S(1)}, bf16[256,2048]{1,0:T(8,128)(2,1)}, u32[]{:S(2)}) copy-start(bf16[256,2048]{1,0:T(8,128)(2,1)} %copy-done.1) | copy-start | bytes 3145732
  227.5 41.6 %all-to-all-start.2 = ((bf16[4,192,2048]{2,1,0:T(8,128)(2,1)}), bf16[4,192,2048]{2,1,0:T(8,128)(2,1)}, u32[]{:S(2)}, u32[]{:S(2)}) async-start(bf16[4,192,2048]{2,1,0:T(8,128)(2,1)} %bitcast.158), calls=%async_computation.2 | async-start | bytes 6291456 | tf_op jit(solution)/shard_map/all_to_all | solution.py:170
Sparse Core Ops, SparseCore 0:
  8.9 50.5 all-gather.6
  61.1 45.9 all-gather.8
  108.8 58.4 all-gather.10
  168.7 46.2 all-gather.12
where the time goes:
time: 305 us; the launch traced here: 304 us
  waiting for transfers between devices  97.1 us (32%)
  local copies, waits for them, and re-layouts  80.6 us (26%)
  matrix products  53 us (17%)
  other arithmetic  24.5 us (8%)
  blocking collectives  19.4 us (6%)
  starting transfers between devices  14.6 us (5%)
  between operations  14.1 us (5%)
    all_to_all x1, waiting for transfers between devices, on_device(): lax.all_to_all(outgoing, 'sp', split_axis=0, concat_axis=0, tiled=True)  36.7 us
    all_to_all x1, waiting for transfers between devices, on_device(): lax.all_to_all(processed, 'sp', split_axis=0, concat_axis=0, tiled=True)  33.3 us
    dynamic_update_slice x8, local copies, waits for them, and re-layouts, block_pass(): lax.scan(advance, state, (query_blocks, key_blocks, value_blocks, decay_b...  25.7 us
    all_to_all x1, waiting for transfers between devices, on_device(): lax.all_to_all(ret_rows, 'tp', split_axis=0, concat_axis=1, tiled=True)  20.6 us
    unnamed x32, local copies, waits for them, and re-layouts  13 us
    dot_general x1, matrix products, on_device(): lax.dot_general(middle, down_full, (((1,), (1,)), ((), ())), preferred_el...  12.5 us
    unnamed x1, blocking collectives  11.4 us
    reduce_sum x1, other arithmetic, on_device(): jnp.sum(decay_weighted.reshape(token_count, chosen_count, model_width), a...  10.1 us
  transfers between devices with their start and end apart: 7, of which 4 were waited for; matrix products, arithmetic and copies ran while one was open for 38% of the time, Pallas kernels for 0%

commit v1 on v0

v1 whole, which is shorter than its diff:
```python
import functools

import jax
import jax.numpy as jnp
from jax import lax
from jax.experimental import pallas as pl
from jax.experimental.pallas import tpu as pltpu
from jax.sharding import PartitionSpec as P

HEAD = 64
BLOCK = 256
EXTRA = 8


eps = 1e-05
F32 = jnp.float32
BF16 = jnp.bfloat16


def split(value):
    high = value.astype(BF16)
    return high, (value - high.astype(F32)).astype(BF16)


def per_head(columns, lanes):
    heads = columns.shape[1]
    out = jnp.broadcast_to(columns[:, 0:1], lanes.shape)
    for head in range(1, heads):
        out = jnp.where(lanes // HEAD == head, columns[:, head : head + 1], out)
    return out


def gathered_update(keys, values, column, lanes, end):
    scale = HEAD ** (-0.5)
    weighted = keys.astype(F32) * (jnp.exp(per_head(end - column, lanes)) * scale)
    high, low = split(weighted)
    dims = (((0,), (0,)), ((), ()))
    return lax.dot_general(high, values, dims, preferred_element_type=F32) + lax.dot_general(
        low, values, dims, preferred_element_type=F32
    )


def state_kernel(key_ref, value_ref, column_ref, out_ref):
    width = key_ref.shape[1]
    step = pl.program_id(0)

    @pl.when(step == 0)
    def _():
        out_ref[0:width, :] = jnp.zeros((width, width), F32)
        out_ref[width:, :] = jnp.zeros((EXTRA, width), F32)

    lanes = lax.broadcasted_iota(jnp.int32, key_ref.shape, 1)
    column = column_ref[...]
    end = column[BLOCK - 1 : BLOCK, :]
    end_lanes = per_head(end, lanes[0:1, :])
    fresh = gathered_update(key_ref[...], value_ref[...], column, lanes, end)
    out_ref[0:width, :] = out_ref[0:width, :] * jnp.exp(end_lanes) + fresh
    out_ref[width:, :] = out_ref[width:, :] + end_lanes


def retention_kernel(
    mine_ref, query_ref, key_ref, value_ref, gate_ref, column_ref, row_ref, gain_ref, states_ref,
    out_ref, state
):
    rows, width = query_ref.shape
    heads = width // HEAD
    step = pl.program_id(0)
    count = states_ref.shape[0]
    row_ids = lax.broadcasted_iota(jnp.int32, (width, width), 0) // HEAD
    column_ids = lax.broadcasted_iota(jnp.int32, (width, width), 1) // HEAD

    @pl.when(step == 0)
    def _():
        total = jnp.zeros((width, width), F32)
        for position in range(count - 1):
            decay = jnp.exp(states_ref[position, width : width + 1, :])
            longer = total * decay + states_ref[position, 0:width, :]
            total = jnp.where(position < mine_ref[0], longer, total)
        state[...] = jnp.where(row_ids == column_ids, total, 0.0)

    lanes = lax.broadcasted_iota(jnp.int32, (rows, width), 1)
    queries, keys, values = query_ref[...], key_ref[...], value_ref[...]
    column = column_ref[...]
    end = column[rows - 1 : rows, :]
    causal = lax.broadcasted_iota(jnp.int32, (rows, rows), 0) >= lax.broadcasted_iota(
        jnp.int32, (rows, rows), 1
    )
    scale = HEAD ** (-0.5)
    high, low = split(state[...])
    carried = jnp.dot(queries, high, preferred_element_type=F32) + jnp.dot(
        queries, low, preferred_element_type=F32
    )
    retained = carried * jnp.exp(per_head(column, lanes))
    inner = None
    for head in range(heads):
        own = jnp.where(lanes // HEAD == head, queries.astype(F32), 0.0).astype(BF16)
        scores = lax.dot_general(
            own, keys, (((1,), (1,)), ((), ())), preferred_element_type=F32
        )
        spread = column[:, head : head + 1] - row_ref[0, head : head + 1, :]
        damping = jnp.exp(jnp.where(causal, spread, -jnp.inf))
        factor = (scores * scale * damping).astype(BF16)
        term = jnp.dot(factor, values, preferred_element_type=F32)
        inner = term if inner is None else jnp.where(lanes // HEAD == head, term, inner)
    retained = retained + inner
    fresh = gathered_update(keys, values, column, lanes, end)
    end_lanes = per_head(end, lanes[0:1, :])
    state[...] = state[...] * jnp.exp(end_lanes) + jnp.where(row_ids == column_ids, fresh, 0.0)

    def head_mean(array):
        out = None
        for head in range(heads):
            inside = lanes // HEAD == head
            mean = jnp.sum(jnp.where(inside, array, 0.0), axis=1, keepdims=True) * (1.0 / HEAD)
            out = jnp.broadcast_to(mean, array.shape) if out is None else jnp.where(inside, mean, out)
        return out

    centered = retained - head_mean(retained)
    normed = centered * lax.rsqrt(head_mean(centered * centered) + eps)
    gates = gate_ref[...].astype(F32)
    out_ref[...] = (normed * gain_ref[...] * (gates * jax.nn.sigmoid(gates))).astype(BF16)


def retention(query_rows, key_rows, value_rows, gate_rows, log_decay, head_gain):
    rows, width = query_rows.shape
    heads = width // HEAD
    count = rows // BLOCK
    running = jnp.cumsum(log_decay.reshape(heads, count, BLOCK), axis=2)
    row = running.transpose(1, 0, 2)
    column = running.reshape(heads, rows).T
    block = pl.BlockSpec((BLOCK, width), lambda i: (i, 0))
    column_block = pl.BlockSpec((BLOCK, heads), lambda i: (i, 0))
    own = pl.pallas_call(
        state_kernel,
        grid=(count,),
        in_specs=[block, block, column_block],
        out_specs=pl.BlockSpec((width + EXTRA, width), lambda i: (0, 0)),
        out_shape=jax.ShapeDtypeStruct((width + EXTRA, width), F32),
        compiler_params=pltpu.CompilerParams(dimension_semantics=("arbitrary",)),
        cost_estimate=pl.CostEstimate(
            flops=4 * rows * width * width, bytes_accessed=4 * rows * width, transcendentals=rows * width
        ),
    )(key_rows, value_rows, column)
    states = lax.all_gather(own, "sp")
    mine = lax.axis_index("sp").astype(jnp.int32).reshape(1)
    return pl.pallas_call(
        retention_kernel,
        grid=(count,),
        in_specs=[
            pl.BlockSpec(memory_space=pltpu.SMEM),
            block,
            block,
            block,
            block,
            column_block,
            pl.BlockSpec((1, heads, BLOCK), lambda i: (i, 0, 0)),
            pl.BlockSpec((1, width), lambda i: (0, 0)),
            pl.BlockSpec(states.shape, lambda i: (0, 0, 0)),
        ],
        out_specs=block,
        out_shape=jax.ShapeDtypeStruct((rows, width), BF16),
        scratch_shapes=[pltpu.VMEM((width, width), F32)],
        compiler_params=pltpu.CompilerParams(dimension_semantics=("arbitrary",)),
        cost_estimate=pl.CostEstimate(
            flops=8 * rows * width * BLOCK,
            bytes_accessed=10 * rows * width,
            transcendentals=rows * BLOCK * heads,
        ),
    )(mine, query_rows, key_rows, value_rows, gate_rows, column, row, head_gain[None, :], states)


def both_halves(weight):
    size = lax.axis_size("tp")
    groups = [list(range(core, size, 2)) for core in range(2)]
    half = lax.all_gather(weight, "tp", axis=1, tiled=True, axis_index_groups=groups)
    other = lax.ppermute(half, "tp", [(i, i ^ 1) for i in range(size)])
    return half, other


def on_device(
    query_rows,
    key_rows,
    value_rows,
    gate_rows,
    log_decay,
    residual,
    head_gain,
    out_weight,
    norm_gain,
    expert_ids,
    route_weights,
    expert_gate,
    expert_up,
    expert_down,
    shared_gate,
    shared_up,
    shared_down,
):
    out_half, out_other = both_halves(out_weight)
    gates, ups, downs = both_halves(expert_gate), both_halves(expert_up), both_halves(expert_down)

    specialists = lax.axis_size("sp")
    tokens, chosen = expert_ids.shape
    width = residual.shape[1]
    capacity = 3 * tokens * chosen // (2 * specialists)
    names = jnp.arange(specialists, dtype=jnp.int32)[:, None]
    named = [expert_ids[:, j][None, :] == names for j in range(chosen)]
    match = functools.reduce(jnp.logical_or, named)
    weight = sum(jnp.where(named[j], route_weights[:, j][None, :], 0.0) for j in range(chosen))
    earlier = jnp.arange(tokens)[:, None] < jnp.arange(tokens)[None, :]
    position = jnp.dot(match.astype(BF16), earlier.astype(BF16), preferred_element_type=F32)
    place = jnp.where(match, position.astype(jnp.int32), -1)
    sits = place[:, None, :] == jnp.arange(capacity, dtype=jnp.int32)[None, :, None]
    pick = sits.astype(BF16).reshape(specialists * capacity, tokens)
    weight_high = lax.reduce_precision(weight, 8, 7)
    weight_low = weight - weight_high
    back_high = jnp.where(sits, weight_high[:, None, :], 0.0).astype(BF16)
    back_low = jnp.where(sits, weight_low[:, None, :], 0.0).astype(BF16)

    ret_rows = retention(query_rows, key_rows, value_rows, gate_rows, log_decay, head_gain)
    token_rows = lax.all_to_all(ret_rows, "tp", split_axis=0, concat_axis=1, tiled=True)
    mine = jnp.dot(token_rows, out_half, preferred_element_type=F32)
    others = jnp.dot(token_rows, out_other, preferred_element_type=F32)
    core = lax.axis_index("tp") % 2
    piece = out_weight.shape[1]
    mine, others = mine.reshape(tokens, -1, piece), others.reshape(tokens, -1, piece)
    mixer = jnp.stack(
        [jnp.where(core == 0, mine, others), jnp.where(core == 0, others, mine)], axis=2
    ).reshape(tokens, width)
    hidden = (residual.astype(F32) + mixer).astype(BF16)
    hidden_wide = hidden.astype(F32)
    normed_rows = (
        hidden_wide
        * lax.rsqrt(jnp.mean(hidden_wide * hidden_wide, axis=1, keepdims=True) + eps)
        * norm_gain
    ).astype(BF16)
    outgoing = jnp.dot(pick, normed_rows, preferred_element_type=F32).astype(BF16)
    outgoing = outgoing.reshape(specialists, capacity, width)
    arrived = lax.all_to_all(outgoing, "sp", split_axis=0, concat_axis=0, tiled=True)
    shared_mid = (
        jax.nn.silu(jnp.dot(normed_rows, shared_gate, preferred_element_type=F32))
        * jnp.dot(normed_rows, shared_up, preferred_element_type=F32)
    ).astype(BF16)
    shared_out = lax.dot_general(
        shared_mid, shared_down, (((1,), (1,)), ((), ())), preferred_element_type=F32
    )
    flat_rows = arrived.reshape(-1, width)
    outcome = 0.0
    for gate, up, down in zip(gates, ups, downs):
        middle = (
            jax.nn.silu(jnp.dot(flat_rows, gate, preferred_element_type=F32))
            * jnp.dot(flat_rows, up, preferred_element_type=F32)
        ).astype(BF16)
        outcome += lax.dot_general(
            middle, down, (((1,), (1,)), ((), ())), preferred_element_type=F32
        )
    processed = outcome.astype(BF16).reshape(arrived.shape)
    returned = lax.all_to_all(processed, "sp", split_axis=0, concat_axis=0, tiled=True)
    dims = (((0, 1), (0, 1)), ((), ()))
    routed = lax.dot_general(back_high, returned, dims, preferred_element_type=F32)
    routed += lax.dot_general(back_low, returned, dims, preferred_element_type=F32)
    return (hidden_wide + routed + shared_out).astype(BF16)


def solution(mesh):
    placed = (
        P("sp", "tp"),
        P("sp", "tp"),
        P("sp", "tp"),
        P("sp", "tp"),
        P("tp", "sp"),
        P(("sp", "tp"), None),
        P("tp"),
        P(None, "tp"),
        P(),
        P(("sp", "tp"), None),
        P(("sp", "tp"), None),
        P(None, ("sp", "tp")),
        P(None, ("sp", "tp")),
        P(None, ("sp", "tp")),
        P(),
        P(),
        P(),
    )
    return jax.shard_map(
        on_device, mesh=mesh, in_specs=placed, out_specs=P(("sp", "tp"), None), check_vma=False
    )
```

time: 305 us -> 300 us (0.984)
  waiting for transfers between devices: 97.1 us -> 171 us
  local copies, waits for them, and re-layouts: 80.6 us -> 15.9 us
  other arithmetic: 24.5 us -> 3.89 us
  Pallas kernels: 0 us -> 14.9 us
  blocking collectives: 19.4 us -> 10.9 us
    all_gather x4, waiting for transfers between devices: 3.96 us -> 112 us  [both_halves(): lax.all_gather(weight, 'tp', axis=1, tiled=True, axis_index_groups=groups)]
    all_to_all x1, waiting for transfers between devices: 36.7 us -> 0.01 us  [on_device(): lax.all_to_all(outgoing, 'sp', split_axis=0, concat_axis=0, tiled=True)]
    dynamic_update_slice x8 -> x0, local copies, waits for them, and re-layouts: 25.7 us -> none  [block_pass(): lax.scan(advance, state, (query_blocks, key_blocks, value_blocks, decay_b...]
    pallas_call x0 -> x2, Pallas kernels: none -> 14.9 us  [the longest x1 8.3 us: retention(): pl.pallas_call(retention_kernel, grid=(count,), in_specs=[pl.BlockSpec(me...]
    unnamed x32 -> x8, local copies, waits for them, and re-layouts: 13 us -> 0.02 us
    gather x2 -> x0, local copies, waits for them, and re-layouts: 11.9 us -> none  [the longest x1 7.56 us: on_device(): returned.reshape(specialist_networks * capacity, model_width)[slot]]
    unnamed x1 -> x0, blocking collectives: 11.4 us -> none
    reduce_sum x3 -> x1, other arithmetic: 10.3 us -> 2.28 us  [on_device(): jnp.mean(hidden_wide * hidden_wide, axis=1, keepdims=True) + eps]
  transfers between devices with their start and end apart: 7 -> 11, of which waited for: 4 -> 5; matrix products, arithmetic and copies ran while one was open for 38% -> 18% of each run, Pallas kernels for 0% -> 5%
where the time goes in v1:
time: 300 us; the launch traced here: 299 us
  waiting for transfers between devices  171 us (57%)
  matrix products  55.3 us (18%)
  local copies, waits for them, and re-layouts  15.9 us (5%)
  Pallas kernels  14.9 us (5%)
  starting transfers between devices  13.5 us (4%)
  between operations  13.3 us (4%)
  blocking collectives  10.9 us (4%)
  other arithmetic  3.89 us (1%)
    all_gather x4, waiting for transfers between devices, both_halves(): lax.all_gather(weight, 'tp', axis=1, tiled=True, axis_index_groups=groups)  112 us
    all_to_all x1, waiting for transfers between devices, on_device(): lax.all_to_all(processed, 'sp', split_axis=0, concat_axis=0, tiled=True)  33.9 us
    all_to_all x1, waiting for transfers between devices, on_device(): lax.all_to_all(ret_rows, 'tp', split_axis=0, concat_axis=1, tiled=True)  22.5 us
    dot_general x2, matrix products, on_device(): lax.dot_general(middle, down, (((1,), (1,)), ((), ())), preferred_element...  20.3 us
    dot_general x2, matrix products, on_device(): jnp.dot(flat_rows, gate, preferred_element_type=F32)  11 us
    all_gather x1, blocking collectives, retention(): states = lax.all_gather(own, 'sp')  10.9 us
    pallas_call x1, Pallas kernels, retention(): pl.pallas_call(retention_kernel, grid=(count,), in_specs=[pl.BlockSpec(me...  8.3 us
    pallas_call x1, Pallas kernels, retention(): pl.pallas_call(state_kernel, grid=(count,), in_specs=[block, block, colum...  6.63 us
  transfers between devices with their start and end apart: 11, of which 5 were waited for; matrix products, arithmetic and copies ran while one was open for 18% of the time, Pallas kernels for 5%

profile of v1, /device:TPU:0, one launch (start us, length us, event | category | flops | bytes accessed | tf_op | source)
XLA Modules:
  0.0 298.8 jit_solution(6322306928654654553)
XLA Ops:
  8.7 49.2 %all-gather.6.cloned.1.call-done = bf16[1024,1024]{1,0:T(8,128)(2,1)} async-done(((bf16[1024,256]{1,0:T(8,128)(2,1)}), bf16[1024,1024]{1,0:T(8,128)(2,1)}) %all-gather.6.cloned.1.call-update) | async-done | bytes 2097168 | tf_op jit(solution)/shard_map/all_gather | solution.py:175
  62.1 6.6 %shard_map.163 = f32[136,128]{1,0:T(8,128)} custom-call(bf16[2048,128]{1,0:T(8,128)(2,1)} %key_ref.3, bf16[2048,128]{1,0:T(8,128)(2,1)} %value_ref.3, f32[2048,2]{1,0:T(8,128)} %bitcast.58), custom_call_target="tpu_custom_call" | custom-call | flops 134217728 | bytes 1048576 | tf_op jit(solution)/shard_map/pallas_call | solution.py:133
  68.7 10.9 %all-gather = f32[544,128]{1,0:T(8,128)} all-gather(f32[136,128]{1,0:T(8,128)} %shard_map.163), channel_id=2, replica_groups=mesh['sp'=4,'tp'=8] {'sp'}, dimensions={0}, use_global_device_ids=true | all-gather | bytes 348160 | tf_op jit(solution)/shard_map/all_gather | solution.py:144
  79.6 8.3 %shard_map.164 = bf16[2048,128]{1,0:T(8,128)(2,1)} custom-call(s32[1]{0:T(128)} %bitcast.mine_ref, bf16[2048,128]{1,0:T(8,128)(2,1)} %query_ref.1, bf16[2048,128]{1,0:T(8,128)(2,1)} %key_ref.3, bf16[2048,128]{1,0:T(8,128)(2,1)} %value_ref.3, bf16[2048,128]{1,0:T(8,128)(2,1)} %gate_ref.1, f32[2048,2]{1,0:T(8,128)} %bitcast.59, f32[8,2,256]{2,1,0:T(2,128)} %bitcast.68, ...), custom_call_target="tpu_custom_call" | custom-call | flops 536870912 | bytes 2621440 | tf_op jit(solution)/shard_map/pallas_call | solution.py:146
  87.9 3.5 %all-to-all-start = ((bf16[8,256,128]{2,1,0:T(8,128)(2,1)}), bf16[8,256,128]{2,1,0:T(8,128)(2,1)S(1)}, u32[]{:S(2)}, u32[]{:S(2)}) async-start(bf16[8,256,128]{2,1,0:T(8,128)(2,1)} %bitcast.64), calls=%async_computation | async-start | bytes 1048576 | tf_op jit(solution)/shard_map/all_to_all | solution.py:221
  92.4 22.5 %all-to-all-done = bf16[8,256,128]{2,1,0:T(8,128)(2,1)S(1)} async-done(((bf16[8,256,128]{2,1,0:T(8,128)(2,1)}), bf16[8,256,128]{2,1,0:T(8,128)(2,1)S(1)}, u32[]{:S(2)}, u32[]{:S(2)}) %all-to-all-start) | async-done | bytes 524320 | tf_op jit(solution)/shard_map/all_to_all | solution.py:221
  115.5 4.0 %copy.28 = bf16[1024,1024]{1,0:T(8,128)(2,1)} copy(bf16[1024,1024]{0,1:T(8,128)(2,1)} %bitcast.65) | data formatting | bytes 4194304 | tf_op jit(solution)/shard_map/dot_general | solution.py:222
  119.5 3.3 %fusion.42 = f32[256,4,256]{0,2,1:T(8,128)} fusion(bf16[256,1024,1]{1,0,2:T(8,128)(2,1)S(1)} %reshape.193, bf16[4,256,1024]{2,1,0:T(8,128)(2,1)} %bitcast.61), kind=kOutput, calls=%fused_computation.63 | convolution fusion | flops 536870912 | bytes 3670016 | tf_op jit(solution)/shard_map/dot_general | solution.py:222
  122.8 4.0 %copy.29 = bf16[1024,1024]{1,0:T(8,128)(2,1)} copy(bf16[1024,1024]{0,1:T(8,128)(2,1)} %bitcast.11) | data formatting | bytes 4194304 | tf_op jit(solution)/shard_map/dot_general | solution.py:223
  131.0 2.9 copy.31
  136.2 2.8 convolution_convert_fusion
  139.0 4.9 %all-to-all-start.1 = ((bf16[4,192,2048]{2,1,0:T(8,128)(2,1)}), bf16[4,192,2048]{2,1,0:T(8,128)(2,1)}, u32[]{:S(2)}, u32[]{:S(2)}) async-start(bf16[4,192,2048]{2,1,0:T(8,128)(2,1)} %bitcast.57), calls=%async_computation.1 | async-start | bytes 6291456 | tf_op jit(solution)/shard_map/all_to_all | solution.py:239
  144.2 17.0 %all-gather.10.cloned.1.call-done = bf16[2048,512]{1,0:T(8,128)(2,1)} async-done(((bf16[2048,128]{1,0:T(8,128)(2,1)}), bf16[2048,512]{1,0:T(8,128)(2,1)}) %all-gather.10.cloned.1.call-update) | async-done | bytes 2097168 | tf_op jit(solution)/shard_map/all_gather | solution.py:175
  161.2 45.9 %all-gather.12.cloned.1.call-done = bf16[2048,512]{1,0:T(8,128)(2,1)} async-done(((bf16[2048,128]{1,0:T(8,128)(2,1)}), bf16[2048,512]{1,0:T(8,128)(2,1)}) %all-gather.12.cloned.1.call-update) | async-done | bytes 2097168 | tf_op jit(solution)/shard_map/all_gather | solution.py:175
  207.1 5.5 %fusion.43 = f32[768,512]{1,0:T(8,128)} fusion(bf16[768,2048]{1,0:T(8,128)(2,1)} %bitcast.22, bf16[2048,512]{1,0:T(8,128)(2,1)} %all-gather.8.cloned.1.call-done), kind=kOutput, calls=%fused_computation.64 | convolution fusion | flops 1610612736 | bytes 6815744 | tf_op jit(solution)/shard_map/dot_general | solution.py:251
  212.6 5.5 %fusion.44 = f32[768,512]{1,0:T(8,128)} fusion(bf16[768,2048]{1,0:T(8,128)(2,1)} %bitcast.22, bf16[2048,512]{1,0:T(8,128)(2,1)} %collective-permute-done.1), kind=kOutput, calls=%fused_computation.65 | convolution fusion | flops 1610612736 | bytes 6815744 | tf_op jit(solution)/shard_map/dot_general | solution.py:251
  218.1 9.8 %fusion.7 = f32[768,2048]{1,0:T(8,128)} fusion(bf16[2048,512]{1,0:T(8,128)(2,1)} %all-gather.12.cloned.1.call-done, f32[768,512]{1,0:T(8,128)} %fusion.43, bf16[768,2048]{1,0:T(8,128)(2,1)} %bitcast.22, bf16[2048,512]{1,0:T(8,128)(2,1)} %all-gather.10.cloned.1.call-done), kind=kOutput, calls=%fused_computation.23 | convolution fusion | flops 3223584768 | bytes 15204352 | tf_op jit(solution)/shard_map/dot_general | solution.py:254
  227.9 10.6 %add_convert_fusion = bf16[768,2048]{1,0:T(8,128)(2,1)} fusion(f32[768,2048]{1,0:T(8,128)} %fusion.7, bf16[2048,512]{1,0:T(8,128)(2,1)} %collective-permute-done.3, f32[768,512]{1,0:T(8,128)} %fusion.44, bf16[768,2048]{1,0:T(8,128)(2,1)} %bitcast.22, bf16[2048,512]{1,0:T(8,128)(2,1)} %collective-permute-done.2), kind=kOutput, calls=%fused_computation | convolution fusion | flops 3226730496 | bytes 18350080 | tf_op jit(solution)/shard_map/dot_general | solution.py:254
  238.5 4.8 %all-to-all-start.2 = ((bf16[4,192,2048]{2,1,0:T(8,128)(2,1)}), bf16[4,192,2048]{2,1,0:T(8,128)(2,1)}, u32[]{:S(2)}, u32[]{:S(2)}) async-start(bf16[4,192,2048]{2,1,0:T(8,128)(2,1)} %bitcast.63), calls=%async_computation.2 | async-start | bytes 6291456 | tf_op jit(solution)/shard_map/all_to_all | solution.py:258
  243.3 3.2 %fusion.35 = f32[256,512]{1,0:T(8,128)} fusion(bf16[2048,512]{1,0:T(8,128)(2,1)} %param.31, bf16[256,2048]{1,0:T(8,128)(2,1)S(1)} %get-tuple-element.6, f32[2048]{0:T(1024)S(1)} %copy-done.1, f32[256]{0:T(256)S(1)} %add_rsqrt_fusion), kind=kOutput, calls=%fused_computation.59 | convolution fusion | flops 538968064 | bytes 3679232 | tf_op jit(solution)/shard_map/dot_general | solution.py:241
  246.5 33.9 %all-to-all-done.2 = bf16[4,192,2048]{2,1,0:T(8,128)(2,1)} async-done(((bf16[4,192,2048]{2,1,0:T(8,128)(2,1)}), bf16[4,192,2048]{2,1,0:T(8,128)(2,1)}, u32[]{:S(2)}, u32[]{:S(2)}) %all-to-all-start.2) | async-done | bytes 3145760 | tf_op jit(solution)/shard_map/all_to_all | solution.py:258
  280.3 2.9 convolution_bitcast_fusion
  283.2 4.3 %convert_add_fusion = f32[256,2048]{1,0:T(8,128)} fusion(bf16[256,2048]{1,0:T(8,128)(2,1)S(1)} %get-tuple-element.6, f32[256,2048]{1,0:T(8,128)S(1)} %convolution_bitcast_fusion, bf16[4,192,2048]{2,1,0:T(8,128)(2,1)} %all-to-all-done.2, bf16[4,256]{1,0:T(4,128)(2,1)S(1)} %get-tuple-element.9, s32[4,256]{1,0:T(4,128)S(1)} %fusion.6), kind=kOutput, calls=%fused_computation.2 | convolution fusion | flops 807272448 | bytes 8394752 | tf_op jit(solution)/shard_map/dot_general | solution.py:260
  287.5 4.8 %fusion.1 = bf16[256,2048]{1,0:T(8,128)(2,1)} fusion(f32[256,2048]{1,0:T(8,128)} %convert_add_fusion, bf16[2048,512]{1,0:T(8,128)(2,1)S(1)} %copy-done, bf16[2048,512]{1,0:T(8,128)(2,1)} %param.32, f32[256,512]{1,0:T(8,128)} %fusion.35, bf16[256,2048]{1,0:T(8,128)(2,1)S(1)} %get-tuple-element.6, f32[2048]{0:T(1024)S(1)} %copy-done.1, f32[256]{0:T(256)S(1)} %add_rsqrt_fusion), kind=kOutput, calls=%fused_computation.9 | convolution fusion | flops 1077673984 | bytes 8922112 | tf_op jit(solution)/shard_map/dot_general | solution.py:244
  (50 shorter events, 14.7 us)
Async XLA Ops:
  6.5 281.0 %copy-start = (bf16[2048,512]{1,0:T(8,128)(2,1)S(1)}, bf16[2048,512]{1,0:T(8,128)(2,1)}, u32[]{:S(2)}) copy-start(bf16[2048,512]{1,0:T(8,128)(2,1)} %param.33) | copy-start | bytes 6291460
  6.5 51.4 %all-gather.6.cloned.1.call-start = ((), (), s32[]{:S(2)}) async-start(), calls=%async_computation.3 | async-start | bytes 2621440 | tf_op jit(solution)/shard_map/all_gather | solution.py:175
  7.3 136.6 %all-gather.8.cloned.1.call-start = ((), (), s32[]{:S(2)}) async-start(), calls=%async_computation.4 | async-start | bytes 2621440 | tf_op jit(solution)/shard_map/all_gather | solution.py:175
  8.0 153.2 %all-gather.10.cloned.1.call-start = ((), (), s32[]{:S(2)}) async-start(), calls=%async_computation.5 | async-start | bytes 2621440 | tf_op jit(solution)/shard_map/all_gather | solution.py:175
  57.9 64.9 %collective-permute-start = (bf16[1024,1024]{1,0:T(8,128)(2,1)}, bf16[1024,1024]{1,0:T(8,128)(2,1)}, u32[]{:S(2)}, u32[]{:S(2)}) collective-permute-start(bf16[1024,1024]{1,0:T(8,128)(2,1)} %all-gather.6.cloned.1.call-done), channel_id=1, source_target_pairs={{0,1},{1,0},{2,3},{3,2},{4,5},{5,4},{6,7},{7,6},{8,9},{9,8},{10,11... | collective-permute-start | bytes 6291464 | tf_op jit(solution)/shard_map/ppermute | solution.py:176
  79.6 12.5 %copy-start.2 = (s32[256,2]{0,1:T(2,128)S(1)}, s32[256,2]{0,1:T(2,128)}, u32[]{:S(2)}) copy-start(s32[256,2]{0,1:T(2,128)} %param.26) | copy-start | bytes 6148
  87.9 27.0 %all-to-all-start = ((bf16[8,256,128]{2,1,0:T(8,128)(2,1)}), bf16[8,256,128]{2,1,0:T(8,128)(2,1)S(1)}, u32[]{:S(2)}, u32[]{:S(2)}) async-start(bf16[8,256,128]{2,1,0:T(8,128)(2,1)} %bitcast.64), calls=%async_computation | async-start | bytes 1048576 | tf_op jit(solution)/shard_map/all_to_all | solution.py:221
  91.4 115.7 %all-gather.12.cloned.1.call-start = ((), (), s32[]{:S(2)}) async-start(), calls=%async_computation.6 | async-start | bytes 2621440 | tf_op jit(solution)/shard_map/all_gather | solution.py:175
  133.9 2.3 copy-start.1
  139.0 68.1 %all-to-all-start.1 = ((bf16[4,192,2048]{2,1,0:T(8,128)(2,1)}), bf16[4,192,2048]{2,1,0:T(8,128)(2,1)}, u32[]{:S(2)}, u32[]{:S(2)}) async-start(bf16[4,192,2048]{2,1,0:T(8,128)(2,1)} %bitcast.57), calls=%async_computation.1 | async-start | bytes 6291456 | tf_op jit(solution)/shard_map/all_to_all | solution.py:239
  143.9 68.7 %collective-permute-start.1 = (bf16[2048,512]{1,0:T(8,128)(2,1)}, bf16[2048,512]{1,0:T(8,128)(2,1)}, u32[]{:S(2)}, u32[]{:S(2)}) collective-permute-start(bf16[2048,512]{1,0:T(8,128)(2,1)} %all-gather.8.cloned.1.call-done), channel_id=1, source_target_pairs={{0,1},{1,0},{2,3},{3,2},{4,5},{5,4},{6,7},{7,6},{8,9},{9,8},{10,11... | collective-permute-start | bytes 6291464 | tf_op jit(solution)/shard_map/ppermute | solution.py:176
  161.2 66.7 %collective-permute-start.2 = (bf16[2048,512]{1,0:T(8,128)(2,1)}, bf16[2048,512]{1,0:T(8,128)(2,1)}, u32[]{:S(2)}, u32[]{:S(2)}) collective-permute-start(bf16[2048,512]{1,0:T(8,128)(2,1)} %all-gather.10.cloned.1.call-done), channel_id=1, source_target_pairs={{0,1},{1,0},{2,3},{3,2},{4,5},{5,4},{6,7},{7,6},{8,9},{9,8},{10,11... | collective-permute-start | bytes 6291464 | tf_op jit(solution)/shard_map/ppermute | solution.py:176
  207.1 20.8 %collective-permute-start.3 = (bf16[2048,512]{1,0:T(8,128)(2,1)}, bf16[2048,512]{1,0:T(8,128)(2,1)}, u32[]{:S(2)}, u32[]{:S(2)}) collective-permute-start(bf16[2048,512]{1,0:T(8,128)(2,1)} %all-gather.12.cloned.1.call-done), channel_id=1, source_target_pairs={{0,1},{1,0},{2,3},{3,2},{4,5},{5,4},{6,7},{7,6},{8,9},{9,8},{10,11... | collective-permute-start | bytes 6291464 | tf_op jit(solution)/shard_map/ppermute | solution.py:176
  238.4 4.8 %copy-start.3 = (f32[256,2]{0,1:T(2,128)S(1)}, f32[256,2]{0,1:T(2,128)}, u32[]{:S(2)}) copy-start(f32[256,2]{0,1:T(2,128)} %param.27) | copy-start | bytes 6148
  238.5 41.9 %all-to-all-start.2 = ((bf16[4,192,2048]{2,1,0:T(8,128)(2,1)}), bf16[4,192,2048]{2,1,0:T(8,128)(2,1)}, u32[]{:S(2)}, u32[]{:S(2)}) async-start(bf16[4,192,2048]{2,1,0:T(8,128)(2,1)} %bitcast.63), calls=%async_computation.2 | async-start | bytes 6291456 | tf_op jit(solution)/shard_map/all_to_all | solution.py:258
Sparse Core Ops, SparseCore 0:
  8.9 48.9 all-gather.5
  59.5 55.6 all-gather.7
  116.8 44.3 all-gather.9
  162.6 44.4 all-gather.11

commit v2 on v1

--- a/solution.py
+++ b/solution.py
@@ -6,6 +6,7 @@
 from jax.experimental import pallas as pl
 from jax.experimental.pallas import tpu as pltpu
 from jax.sharding import PartitionSpec as P
+
 
 HEAD = 64
 BLOCK = 256
@@ -130,7 +131,7 @@
     column = running.reshape(heads, rows).T
     block = pl.BlockSpec((BLOCK, width), lambda i: (i, 0))
     column_block = pl.BlockSpec((BLOCK, heads), lambda i: (i, 0))
-    own = pl.pallas_call(
+    state_call = pl.pallas_call(
         state_kernel,
         grid=(count,),
         in_specs=[block, block, column_block],
@@ -140,7 +141,8 @@
         cost_estimate=pl.CostEstimate(
             flops=4 * rows * width * width, bytes_accessed=4 * rows * width, transcendentals=rows * width
         ),
-    )(key_rows, value_rows, column)
+    )
+    own = state_call(key_rows, value_rows, column)
     states = lax.all_gather(own, "sp")
     mine = lax.axis_index("sp").astype(jnp.int32).reshape(1)
     return pl.pallas_call(
@@ -169,12 +171,120 @@
     )(mine, query_rows, key_rows, value_rows, gate_rows, column, row, head_gain[None, :], states)
 
 
-def both_halves(weight):
+def send(piece, pairs):
+    return lax.ppermute(piece, "tp", pairs)
+
+
+def ring_start(own):
     size = lax.axis_size("tp")
-    groups = [list(range(core, size, 2)) for core in range(2)]
-    half = lax.all_gather(weight, "tp", axis=1, tiled=True, axis_index_groups=groups)
-    other = lax.ppermute(half, "tp", [(i, i ^ 1) for i in range(size)])
-    return half, other
+    right = [(i, (i + 2) % size) for i in range(size)]
+    left = [(i, (i - 2) % size) for i in range(size)]
+    swap = [(i, i ^ 1) for i in range(size)]
+    return send(own, right), send(own, left), send(own, swap)
+
+
+def ring_finish(own, from_left, from_right, other):
+    size = lax.axis_size("tp")
+    chips = size // 2
+    right = [(i, (i + 2) % size) for i in range(size)]
+    left = [(i, (i - 2) % size) for i in range(size)]
+    swap = [(i, i ^ 1) for i in range(size)]
+    half = own.shape[1] // 2
+    last = chips // 2
+    pieces = [[own], [other]]
+    for hop in range(1, (chips - 1) // 2 + 1):
+        if hop > 1:
+            from_left = send(from_left, right)
+            from_right = send(from_right, left)
+        for piece in (from_left, from_right):
+            pieces += [[piece], [send(piece, swap)]]
+    if chips % 2 == 0 and last > 1:
+        first = send(from_left[:, :half], right)
+        second = send(from_right[:, half:], left)
+        pieces += [[first, second], [send(first, swap), send(second, swap)]]
+    elif chips == 2:
+        pieces += [[from_left], [send(from_left, swap)]]
+    return pieces
+
+
+def expert_kernel(layout, row_ref, *refs):
+    count = len(layout)
+    piece_refs, out_ref = refs[:count], refs[count]
+    weights, middle, sems = refs[count + 1 :]
+    slots, _, width, ff = weights.shape
+    rows = row_ref.shape[0]
+    copies = []
+    for index, (slot, start, length) in enumerate(layout):
+        copy = pltpu.make_async_copy(
+            piece_refs[index], weights.at[slot, :, pl.ds(start, length), :], sems.at[index]
+        )
+        copy.start()
+        copies.append(copy)
+    tile = rows // 2
+    for pair in range(slots // 2):
+        for index, (slot, _, _) in enumerate(layout):
+            if slot // 2 == pair:
+                copies[index].wait()
+
+        @pl.loop(0, 2)
+        def _(step):
+            span = pl.ds(pl.multiple_of(step * tile, tile), tile)
+            block = row_ref[span, :]
+            gate = jnp.concatenate([weights[2 * pair, 0], weights[2 * pair + 1, 0]], axis=1)
+            up = jnp.concatenate([weights[2 * pair, 1], weights[2 * pair + 1, 1]], axis=1)
+            gated = jnp.dot(block, gate, preferred_element_type=F32)
+            raised = jnp.dot(block, up, preferred_element_type=F32)
+            value = gated * jax.nn.sigmoid(gated) * raised
+            middle[span, 2 * pair * ff : 2 * (pair + 1) * ff] = value.astype(BF16)
+
+    part = 512
+
+    @pl.loop(0, width // part)
+    def _(step):
+        span = pl.ds(pl.multiple_of(step * part, part), part)
+        down = jnp.concatenate([weights[slot, 2, span, :] for slot in range(slots)], axis=1)
+        out_ref[:, span] = lax.dot_general(
+            middle[...], down, (((1,), (1,)), ((), ())), preferred_element_type=F32
+        ).astype(BF16)
+
+
+def experts(rows, shards):
+    _, width, ff = shards[0][0].shape
+    count = len(shards)
+    if ff % 128 or count % 2:
+        whole = jnp.concatenate([jnp.concatenate(shard, axis=1) for shard in shards], axis=2)
+        middle = (
+            jax.nn.silu(jnp.dot(rows, whole[0], preferred_element_type=F32))
+            * jnp.dot(rows, whole[1], preferred_element_type=F32)
+        ).astype(BF16)
+        return lax.dot_general(
+            middle, whole[2], (((1,), (1,)), ((), ())), preferred_element_type=F32
+        ).astype(BF16)
+    layout, pieces = [], []
+    for slot, shard in enumerate(shards):
+        start = 0
+        for piece in shard:
+            layout.append((slot, start, piece.shape[1]))
+            pieces.append(piece)
+            start += piece.shape[1]
+    return pl.pallas_call(
+        functools.partial(expert_kernel, layout),
+        in_specs=[pl.BlockSpec(memory_space=pltpu.VMEM)]
+        + [pl.BlockSpec(memory_space=pl.ANY)] * len(pieces),
+        out_specs=pl.BlockSpec(memory_space=pltpu.VMEM),
+        out_shape=jax.ShapeDtypeStruct(rows.shape, BF16),
+        scratch_shapes=[
+            pltpu.VMEM((count, 3, width, ff), BF16),
+            pltpu.VMEM((rows.shape[0], count * ff), BF16),
+            pltpu.SemaphoreType.DMA((len(pieces),)),
+        ],
+        compiler_params=pltpu.CompilerParams(vmem_limit_bytes=60 * 1024 * 1024),
+        cost_estimate=pl.CostEstimate(
+            flops=6 * rows.shape[0] * width * count * ff,
+            bytes_accessed=6 * width * count * ff + 4 * rows.size,
+            transcendentals=rows.shape[0] * count * ff,
+        ),
+    )(rows, *pieces)
 
 
 def on_device(
@@ -196,8 +306,10 @@
     shared_up,
     shared_down,
 ):
-    out_half, out_other = both_halves(out_weight)
-    gates, ups, downs = both_halves(expert_gate), both_halves(expert_up), both_halves(expert_down)
+    out_full = lax.all_gather(out_weight, "tp", axis=1, tiled=True)
+    shard = jnp.stack([expert_gate, expert_up, expert_down])
+    shard, log_decay = lax.optimization_barrier((shard, log_decay))
+    from_left, from_right, other = ring_start(shard)
 
     specialists = lax.axis_size("sp")
     tokens, chosen = expert_ids.shape
@@ -219,14 +331,9 @@
 
     ret_rows = retention(query_rows, key_rows, value_rows, gate_rows, log_decay, head_gain)
     token_rows = lax.all_to_all(ret_rows, "tp", split_axis=0, concat_axis=1, tiled=True)
-    mine = jnp.dot(token_rows, out_half, preferred_element_type=F32)
-    others = jnp.dot(token_rows, out_other, preferred_element_type=F32)
-    core = lax.axis_index("tp") % 2
-    piece = out_weight.shape[1]
-    mine, others = mine.reshape(tokens, -1, piece), others.reshape(tokens, -1, piece)
-    mixer = jnp.stack(
-        [jnp.where(core == 0, mine, others), jnp.where(core == 0, others, mine)], axis=2
-    ).reshape(tokens, width)
+    token_rows, from_left, from_right = lax.optimization_barrier((token_rows, from_left, from_right))
+    shards = ring_finish(shard, from_left, from_right, other)
+    mixer = jnp.dot(token_rows, out_full, preferred_element_type=F32)
     hidden = (residual.astype(F32) + mixer).astype(BF16)
     hidden_wide = hidden.astype(F32)
     normed_rows = (
@@ -245,16 +352,7 @@
         shared_mid, shared_down, (((1,), (1,)), ((), ())), preferred_element_type=F32
     )
     flat_rows = arrived.reshape(-1, width)
-    outcome = 0.0
-    for gate, up, down in zip(gates, ups, downs):
-        middle = (
-            jax.nn.silu(jnp.dot(flat_rows, gate, preferred_element_type=F32))
-            * jnp.dot(flat_rows, up, preferred_element_type=F32)
-        ).astype(BF16)
-        outcome += lax.dot_general(
-            middle, down, (((1,), (1,)), ((), ())), preferred_element_type=F32
-        )
-    processed = outcome.astype(BF16).reshape(arrived.shape)
+    processed = experts(flat_rows, shards).reshape(arrived.shape)
     returned = lax.all_to_all(processed, "sp", split_axis=0, concat_axis=0, tiled=True)
     dims = (((0, 1), (0, 1)), ((), ()))
     routed = lax.dot_general(back_high, returned, dims, preferred_element_type=F32)
@@ -282,6 +380,7 @@
         P(),
         P(),
     )
+
     return jax.shard_map(
         on_device, mesh=mesh, in_specs=placed, out_specs=P(("sp", "tp"), None), check_vma=False
     )

time: 300 us -> 262 us (0.87)
  matrix products: 55.3 us -> 22.1 us
  waiting for transfers between devices: 171 us -> 146 us
  Pallas kernels: 14.9 us -> 32.4 us
  starting transfers between devices: 13.5 us -> 22.6 us
  local copies, waits for them, and re-layouts: 15.9 us -> 9.25 us
    all_gather x4 -> x1, waiting for transfers between devices: 112 us -> 0.01 us  [on_device(): out_full = lax.all_gather(out_weight, 'tp', axis=1, tiled=True)]
    all_to_all x1, waiting for transfers between devices: 22.5 us -> 77.9 us  [on_device(): lax.all_to_all(ret_rows, 'tp', split_axis=0, concat_axis=1, tiled=True)]
    ppermute x4 -> x9, waiting for transfers between devices: 0.01 us -> 33.9 us  [send(): return lax.ppermute(piece, 'tp', pairs)]
    dot_general x6 -> x1, matrix products: 37.3 us -> 4.06 us  [on_device(): mixer = jnp.dot(token_rows, out_full, preferred_element_type=F32)]
    pallas_call x1 -> x2, Pallas kernels: 6.63 us -> 24.1 us  [the longest x1 17.5 us: experts(): pl.pallas_call(functools.partial(expert_kernel, layout), in_specs=[pl.Blo...]
    ppermute x4 -> x9, starting transfers between devices: 0.27 us -> 9.59 us  [send(): return lax.ppermute(piece, 'tp', pairs)]
    dot_general x2 -> x0, local copies, waits for them, and re-layouts: 7.95 us -> none  [the longest x1 3.99 us: on_device(): others = jnp.dot(token_rows, out_other, preferred_element_type=F32)]
    reshape x3 -> x2, local copies, waits for them, and re-layouts: 3.66 us -> 0.03 us  [the longest x1 2.91 us: on_device(): mixer = jnp.stack([jnp.where(core == 0, mine, others), jnp.where(core ==...]
  transfers between devices with their start and end apart: 11 -> 13, of which waited for: 5 -> 5; matrix products, arithmetic and copies ran while one was open for 18% -> 5% of each run, Pallas kernels for 5% -> 6%
where the time goes in v2:
time: 262 us; the launch traced here: 261 us
  waiting for transfers between devices  146 us (56%)
  Pallas kernels  32.4 us (12%)
  starting transfers between devices  22.6 us (9%)
  matrix products  22.1 us (8%)
  between operations  13.6 us (5%)
  blocking collectives  10.9 us (4%)
  local copies, waits for them, and re-layouts  9.25 us (4%)
  other arithmetic  4.14 us (2%)
    all_to_all x1, waiting for transfers between devices, on_device(): lax.all_to_all(ret_rows, 'tp', split_axis=0, concat_axis=1, tiled=True)  77.9 us
    ppermute x9, waiting for transfers between devices, send(): return lax.ppermute(piece, 'tp', pairs)  33.9 us
    all_to_all x1, waiting for transfers between devices, on_device(): lax.all_to_all(processed, 'sp', split_axis=0, concat_axis=0, tiled=True)  33.7 us
    pallas_call x1, Pallas kernels, experts(): pl.pallas_call(functools.partial(expert_kernel, layout), in_specs=[pl.Blo...  17.5 us
    all_gather x1, blocking collectives, retention(): states = lax.all_gather(own, 'sp')  10.9 us
    ppermute x9, starting transfers between devices, send(): return lax.ppermute(piece, 'tp', pairs)  9.59 us
    pallas_call x1, Pallas kernels, retention(): pl.pallas_call(retention_kernel, grid=(count,), in_specs=[pl.BlockSpec(me...  8.32 us
    pallas_call x1, Pallas kernels, retention(): own = state_call(key_rows, value_rows, column)  6.64 us
  transfers between devices with their start and end apart: 13, of which 5 were waited for; matrix products, arithmetic and copies ran while one was open for 5% of the time, Pallas kernels for 6%

profile of v2, /device:TPU:0, one launch (start us, length us, event | category | flops | bytes accessed | tf_op | source)
XLA Modules:
  0.0 261.2 jit_solution(8848201130064585774)
XLA Ops:
  7.3 2.7 %pad_maximum_fusion.refs_0_ = bf16[3,2048,128]{2,1,0:T(8,128)(2,1)} fusion(bf16[1,2048,128]{2,1,0:T(8,128)(2,1)} %bitcast.48, bf16[1,2048,128]{2,1,0:T(8,128)(2,1)} %bitcast.49, bf16[1,2048,128]{2,1,0:T(8,128)(2,1)} %bitcast.50), kind=kLoop, calls=%fused_computation.14 | loop fusion | flops 1572864 | bytes 3145728 | tf_op jit(solution)/shard_map/stack | solution.py:310
  9.9 3.1 %collective-permute-start = (bf16[3,2048,128]{2,1,0:T(8,128)(2,1)}, bf16[3,2048,128]{2,1,0:T(8,128)(2,1)}, u32[]{:S(2)}, u32[]{:S(2)}) collective-permute-start(bf16[3,2048,128]{2,1,0:T(8,128)(2,1)} %pad_maximum_fusion.refs_0_), channel_id=1, source_target_pairs={{0,2},{1,3},{2,4},{3,5},{4,6},{5,7},{6,0},{7,1},{8,10},{9,11},{10,... | collective-permute-start | bytes 4718600 | tf_op jit(solution)/shard_map/ppermute | solution.py:175
  13.0 2.0 collective-permute-start.1
  16.5 1.4 copy.22
  18.5 6.6 %shard_map.163 = f32[136,128]{1,0:T(8,128)} custom-call(bf16[2048,128]{1,0:T(8,128)(2,1)} %key_ref.3, bf16[2048,128]{1,0:T(8,128)(2,1)} %value_ref.3, f32[2048,2]{1,0:T(8,128)} %bitcast.42), custom_call_target="tpu_custom_call" | custom-call | flops 134217728 | bytes 1048576 | tf_op jit(solution)/shard_map/pallas_call | solution.py:145
  25.1 10.9 %all-gather = f32[544,128]{1,0:T(8,128)} all-gather(f32[136,128]{1,0:T(8,128)} %shard_map.163), channel_id=2, replica_groups=mesh['sp'=4,'tp'=8] {'sp'}, dimensions={0}, use_global_device_ids=true | all-gather | bytes 348160 | tf_op jit(solution)/shard_map/all_gather | solution.py:146
  36.0 8.3 %shard_map.164 = bf16[2048,128]{1,0:T(8,128)(2,1)} custom-call(s32[1]{0:T(128)} %bitcast.mine_ref, bf16[2048,128]{1,0:T(8,128)(2,1)} %query_ref.1, bf16[2048,128]{1,0:T(8,128)(2,1)} %key_ref.3, bf16[2048,128]{1,0:T(8,128)(2,1)} %value_ref.3, bf16[2048,128]{1,0:T(8,128)(2,1)} %gate_ref.1, f32[2048,2]{1,0:T(8,128)} %bitcast.43, f32[8,2,256]{2,1,0:T(2,128)} %bitcast.51, ...), custom_call_target="tpu_custom_call" | custom-call | flops 536870912 | bytes 2621440 | tf_op jit(solution)/shard_map/pallas_call | solution.py:148
  44.4 2.0 copy.24
  46.4 3.5 %all-to-all-start = ((bf16[8,256,128]{1,2,0:T(8,128)(2,1)}), bf16[8,256,128]{1,2,0:T(8,128)(2,1)S(1)}, u32[]{:S(2)}, u32[]{:S(2)}) async-start(bf16[8,256,128]{1,2,0:T(8,128)(2,1)} %copy.24), calls=%async_computation | async-start | bytes 1048576 | tf_op jit(solution)/shard_map/all_to_all | solution.py:333
  50.3 77.9 %all-to-all-done = bf16[8,256,128]{1,2,0:T(8,128)(2,1)S(1)} async-done(((bf16[8,256,128]{1,2,0:T(8,128)(2,1)}), bf16[8,256,128]{1,2,0:T(8,128)(2,1)S(1)}, u32[]{:S(2)}, u32[]{:S(2)}) %all-to-all-start) | async-done | bytes 524320 | tf_op jit(solution)/shard_map/all_to_all | solution.py:333
  129.1 4.1 %fusion.3 = (f32[256]{0:T(256)S(1)}, bf16[256,2048]{1,0:T(8,128)(2,1)S(1)}) fusion(bf16[256,1024]{0,1:T(8,128)(2,1)} %bitcast.47, bf16[1024,2048]{1,0:T(8,128)(2,1)} %all-gather.3.cloned.1.call-done, bf16[256,2048]{1,0:T(8,128)(2,1)} %param.22), kind=kOutput, calls=%fused_computation.11 | convolution fusion | flops 1076887296 | bytes 6816768 | tf_op jit(solution)/shard_map/dot_general | solution.py:336
  133.1 2.8 %convolution_convert_fusion = bf16[768,2048]{1,0:T(8,128)(2,1)} fusion(pred[768,256]{1,0:T(32,128)(4,1)S(1)} %bitcast_compare_fusion, bf16[256,2048]{1,0:T(8,128)(2,1)S(1)} %get-tuple-element.22, f32[2048]{0:T(1024)S(1)} %copy-done.3, f32[256]{0:T(256)S(1)} %add_rsqrt_fusion), kind=kOutput, calls=%fused_computation | convolution fusion | flops 808976384 | bytes 4400128 | tf_op jit(solution)/shard_map/dot_general | solution.py:344
  135.9 4.7 %all-to-all-start.1 = ((bf16[4,192,2048]{2,1,0:T(8,128)(2,1)}), bf16[4,192,2048]{2,1,0:T(8,128)(2,1)}, u32[]{:S(2)}, u32[]{:S(2)}) async-start(bf16[4,192,2048]{2,1,0:T(8,128)(2,1)} %bitcast.41), calls=%async_computation.1 | async-start | bytes 6291456 | tf_op jit(solution)/shard_map/all_to_all | solution.py:346
  143.1 3.9 %collective-permute-start.6 = (bf16[3,1024,128]{2,1,0:T(8,128)(2,1)S(1)}, bf16[3,1024,128]{2,1,0:T(8,128)(2,1)S(1)}, u32[]{:S(2)}, u32[]{:S(2)}) collective-permute-start(bf16[3,1024,128]{2,1,0:T(8,128)(2,1)S(1)} %slice.31), channel_id=1, source_target_pairs={{0,6},{1,7},{2,0},{3,1},{4,2},{5,3},{6,4},{7,5},{8,14},{9,15},{10,... | collective-permute-start | bytes 2359304 | tf_op jit(solution)/shard_map/ppermute | solution.py:175
  147.5 16.7 %collective-permute-done.5.refs_6_ = bf16[3,1024,128]{2,1,0:T(8,128)(2,1)S(1)} collective-permute-done((bf16[3,1024,128]{2,1,0:T(8,128)(2,1)S(1)}, bf16[3,1024,128]{2,1,0:T(8,128)(2,1)S(1)}, u32[]{:S(2)}, u32[]{:S(2)}) %collective-permute-start.5) | collective-permute-done | bytes 786464 | tf_op jit(solution)/shard_map/ppermute | solution.py:175
  164.2 15.8 %collective-permute-done.6.refs_7_ = bf16[3,1024,128]{2,1,0:T(8,128)(2,1)S(1)} collective-permute-done((bf16[3,1024,128]{2,1,0:T(8,128)(2,1)S(1)}, bf16[3,1024,128]{2,1,0:T(8,128)(2,1)S(1)}, u32[]{:S(2)}, u32[]{:S(2)}) %collective-permute-start.6) | collective-permute-done | bytes 786464 | tf_op jit(solution)/shard_map/ppermute | solution.py:175
  180.9 1.4 collective-permute-done.8.refs_9_
  183.2 17.5 %shard_map.165 = bf16[768,2048]{1,0:T(8,128)(2,1)} custom-call(bf16[768,2048]{1,0:T(8,128)(2,1)} %bitcast.19.row_ref, bf16[3,2048,128]{2,1,0:T(8,128)(2,1)} %pad_maximum_fusion.refs_0_, bf16[3,2048,128]{2,1,0:T(8,128)(2,1)} %collective-permute-done.2.refs_1_, bf16[3,2048,128]{2,1,0:T(8,128)(2,1)} %collective-permute-done.refs_2_, ...), custom_call_target="tpu_custom_call" | custom-call | flops 9663676416 | bytes 18874368 | tf_op jit(solution)/shard_map/pallas_call | solution.py:270
  200.6 4.9 %all-to-all-start.2 = ((bf16[4,192,2048]{2,1,0:T(8,128)(2,1)}), bf16[4,192,2048]{2,1,0:T(8,128)(2,1)}, u32[]{:S(2)}, u32[]{:S(2)}) async-start(bf16[4,192,2048]{2,1,0:T(8,128)(2,1)} %bitcast.44), calls=%async_computation.2 | async-start | bytes 6291456 | tf_op jit(solution)/shard_map/all_to_all | solution.py:356
  205.5 3.1 %fusion.31 = f32[256,512]{1,0:T(8,128)} fusion(bf16[2048,512]{1,0:T(8,128)(2,1)} %param.31, bf16[256,2048]{1,0:T(8,128)(2,1)S(1)} %get-tuple-element.22, f32[2048]{0:T(1024)S(1)} %copy-done.3, f32[256]{0:T(256)S(1)} %add_rsqrt_fusion), kind=kOutput, calls=%fused_computation.50 | convolution fusion | flops 538968064 | bytes 3679232 | tf_op jit(solution)/shard_map/dot_general | solution.py:348
  208.7 33.7 %all-to-all-done.2 = bf16[4,192,2048]{2,1,0:T(8,128)(2,1)} async-done(((bf16[4,192,2048]{2,1,0:T(8,128)(2,1)}), bf16[4,192,2048]{2,1,0:T(8,128)(2,1)}, u32[]{:S(2)}, u32[]{:S(2)}) %all-to-all-start.2) | async-done | bytes 3145760 | tf_op jit(solution)/shard_map/all_to_all | solution.py:356
  242.4 2.9 %convolution_bitcast_fusion = f32[256,2048]{1,0:T(8,128)S(1)} fusion(bf16[4,192,2048]{2,1,0:T(8,128)(2,1)} %all-to-all-done.2, bf16[4,256]{1,0:T(4,128)(2,1)S(1)} %get-tuple-element.16, s32[4,256]{1,0:T(4,128)S(1)} %fusion.7), kind=kOutput, calls=%fused_computation.5 | convolution fusion | flops 805699584 | bytes 5249024 | tf_op jit(solution)/shard_map/dot_general | solution.py:359
  245.3 4.3 %convert_add_fusion = f32[256,2048]{1,0:T(8,128)} fusion(bf16[256,2048]{1,0:T(8,128)(2,1)S(1)} %get-tuple-element.22, f32[256,2048]{1,0:T(8,128)S(1)} %convolution_bitcast_fusion, bf16[4,192,2048]{2,1,0:T(8,128)(2,1)} %all-to-all-done.2, bf16[4,256]{1,0:T(4,128)(2,1)S(1)} %get-tuple-element.15, s32[4,256]{1,0:T(4,128)S(1)} %fusion.7), kind=kOutput, calls=%fused_computation.1 | convolution fusion | flops 807272448 | bytes 8394752 | tf_op jit(solution)/shard_map/dot_general | solution.py:358
  249.6 4.8 %fusion.1 = bf16[256,2048]{1,0:T(8,128)(2,1)} fusion(f32[256,2048]{1,0:T(8,128)} %convert_add_fusion, bf16[2048,512]{1,0:T(8,128)(2,1)S(1)} %copy-done, bf16[2048,512]{1,0:T(8,128)(2,1)} %param.32, f32[256,512]{1,0:T(8,128)} %fusion.31, bf16[256,2048]{1,0:T(8,128)(2,1)S(1)} %get-tuple-element.22, f32[2048]{0:T(1024)S(1)} %copy-done.3, f32[256]{0:T(256)S(1)} %add_rsqrt_fusion), kind=kOutput, calls=%fused_computation.9 | convolution fusion | flops 1077673984 | bytes 8922112 | tf_op jit(solution)/shard_map/dot_general | solution.py:351
  (55 shorter events, 8.9 us)
Async XLA Ops:
  6.5 243.1 %copy-start = (bf16[2048,512]{1,0:T(8,128)(2,1)S(1)}, bf16[2048,512]{1,0:T(8,128)(2,1)}, u32[]{:S(2)}) copy-start(bf16[2048,512]{1,0:T(8,128)(2,1)} %param.33) | copy-start | bytes 6291460
  6.5 8.5 %copy-start.2 = (f32[2,2048]{1,0:T(2,128)S(1)}, f32[2,2048]{1,0:T(2,128)}, u32[]{:S(2)}) copy-start(f32[2,2048]{1,0:T(2,128)} %param.21) | copy-start | bytes 49156
  6.5 122.5 %all-gather.3.cloned.1.call-start = ((), (), s32[]{:S(2)}) async-start(), calls=%async_computation.3 | async-start | bytes 4718592 | tf_op jit(solution)/shard_map/all_gather | solution.py:309
  9.9 118.3 %collective-permute-start = (bf16[3,2048,128]{2,1,0:T(8,128)(2,1)}, bf16[3,2048,128]{2,1,0:T(8,128)(2,1)}, u32[]{:S(2)}, u32[]{:S(2)}) collective-permute-start(bf16[3,2048,128]{2,1,0:T(8,128)(2,1)} %pad_maximum_fusion.refs_0_), channel_id=1, source_target_pairs={{0,2},{1,3},{2,4},{3,5},{4,6},{5,7},{6,0},{7,1},{8,10},{9,11},{10,... | collective-permute-start | bytes 4718600 | tf_op jit(solution)/shard_map/ppermute | solution.py:175
  13.0 115.3 %collective-permute-start.1 = (bf16[3,2048,128]{2,1,0:T(8,128)(2,1)}, bf16[3,2048,128]{2,1,0:T(8,128)(2,1)}, u32[]{:S(2)}, u32[]{:S(2)}) collective-permute-start(bf16[3,2048,128]{2,1,0:T(8,128)(2,1)} %pad_maximum_fusion.refs_0_), channel_id=1, source_target_pairs={{0,6},{1,7},{2,0},{3,1},{4,2},{5,3},{6,4},{7,5},{8,14},{9,15},{10,... | collective-permute-start | bytes 4718600 | tf_op jit(solution)/shard_map/ppermute | solution.py:175
  36.0 14.0 %copy-start.4 = (s32[256,2]{0,1:T(2,128)S(1)}, s32[256,2]{0,1:T(2,128)}, u32[]{:S(2)}) copy-start(s32[256,2]{0,1:T(2,128)} %param.26) | copy-start | bytes 6148
  46.4 81.9 %all-to-all-start = ((bf16[8,256,128]{1,2,0:T(8,128)(2,1)}), bf16[8,256,128]{1,2,0:T(8,128)(2,1)S(1)}, u32[]{:S(2)}, u32[]{:S(2)}) async-start(bf16[8,256,128]{1,2,0:T(8,128)(2,1)} %copy.24), calls=%async_computation | async-start | bytes 1048576 | tf_op jit(solution)/shard_map/all_to_all | solution.py:333
  128.3 0.8 copy-start.1
  129.1 4.1 %copy-start.3 = (f32[2048]{0:T(1024)S(1)}, f32[2048]{0:T(1024)}, u32[]{:S(2)}) copy-start(f32[2048]{0:T(1024)} %param.25) | copy-start | bytes 24580
  135.9 47.2 %all-to-all-start.1 = ((bf16[4,192,2048]{2,1,0:T(8,128)(2,1)}), bf16[4,192,2048]{2,1,0:T(8,128)(2,1)}, u32[]{:S(2)}, u32[]{:S(2)}) async-start(bf16[4,192,2048]{2,1,0:T(8,128)(2,1)} %bitcast.41), calls=%async_computation.1 | async-start | bytes 6291456 | tf_op jit(solution)/shard_map/all_to_all | solution.py:346
  140.6 39.4 %collective-permute-start.2 = (bf16[3,2048,128]{2,1,0:T(8,128)(2,1)}, bf16[3,2048,128]{2,1,0:T(8,128)(2,1)}, u32[]{:S(2)}, u32[]{:S(2)}) collective-permute-start(bf16[3,2048,128]{2,1,0:T(8,128)(2,1)} %pad_maximum_fusion.refs_0_), channel_id=1, source_target_pairs={{0,1},{1,0},{2,3},{3,2},{4,5},{5,4},{6,7},{7,6},{8,9},{9,8},{10,11... | collective-permute-start | bytes 4718600 | tf_op jit(solution)/shard_map/ppermute | solution.py:175
  141.9 22.3 %collective-permute-start.5 = (bf16[3,1024,128]{2,1,0:T(8,128)(2,1)S(1)}, bf16[3,1024,128]{2,1,0:T(8,128)(2,1)S(1)}, u32[]{:S(2)}, u32[]{:S(2)}) collective-permute-start(bf16[3,1024,128]{2,1,0:T(8,128)(2,1)S(1)} %slice.30), channel_id=1, source_target_pairs={{0,2},{1,3},{2,4},{3,5},{4,6},{5,7},{6,0},{7,1},{8,10},{9,11},{10,... | collective-permute-start | bytes 2359304 | tf_op jit(solution)/shard_map/ppermute | solution.py:175
  143.1 36.8 %collective-permute-start.6 = (bf16[3,1024,128]{2,1,0:T(8,128)(2,1)S(1)}, bf16[3,1024,128]{2,1,0:T(8,128)(2,1)S(1)}, u32[]{:S(2)}, u32[]{:S(2)}) collective-permute-start(bf16[3,1024,128]{2,1,0:T(8,128)(2,1)S(1)} %slice.31), channel_id=1, source_target_pairs={{0,6},{1,7},{2,0},{3,1},{4,2},{5,3},{6,4},{7,5},{8,14},{9,15},{10,... | collective-permute-start | bytes 2359304 | tf_op jit(solution)/shard_map/ppermute | solution.py:175
  147.0 35.3 %collective-permute-start.3 = (bf16[3,2048,128]{2,1,0:T(8,128)(2,1)}, bf16[3,2048,128]{2,1,0:T(8,128)(2,1)}, u32[]{:S(2)}, u32[]{:S(2)}) collective-permute-start(bf16[3,2048,128]{2,1,0:T(8,128)(2,1)} %collective-permute-done.refs_2_), channel_id=1, source_target_pairs={{0,1},{1,0},{2,3},{3,2},{4,5},{5,4},{6,7},{7,6},{8,9},{9,8},{10,11... | collective-permute-start | bytes 4718600 | tf_op jit(solution)/shard_map/ppermute | solution.py:175
  147.0 36.2 %collective-permute-start.4 = (bf16[3,2048,128]{2,1,0:T(8,128)(2,1)}, bf16[3,2048,128]{2,1,0:T(8,128)(2,1)}, u32[]{:S(2)}, u32[]{:S(2)}) collective-permute-start(bf16[3,2048,128]{2,1,0:T(8,128)(2,1)} %collective-permute-done.1.refs_4_), channel_id=1, source_target_pairs={{0,1},{1,0},{2,3},{3,2},{4,5},{5,4},{6,7},{7,6},{8,9},{9,8},{10,11... | collective-permute-start | bytes 4718600 | tf_op jit(solution)/shard_map/ppermute | solution.py:175
  164.2 15.8 %copy-start.6 = (bf16[3,1024,128]{2,1,0:T(8,128)(2,1)}, bf16[3,1024,128]{2,1,0:T(8,128)(2,1)S(1)}, u32[]{:S(2)}) copy-start(bf16[3,1024,128]{2,1,0:T(8,128)(2,1)S(1)} %collective-permute-done.5.refs_6_) | copy-start | bytes 2359300
  164.2 15.8 %collective-permute-start.7 = (bf16[3,1024,128]{2,1,0:T(8,128)(2,1)S(1)}, bf16[3,1024,128]{2,1,0:T(8,128)(2,1)S(1)}, u32[]{:S(2)}, u32[]{:S(2)}) collective-permute-start(bf16[3,1024,128]{2,1,0:T(8,128)(2,1)S(1)} %collective-permute-done.5.refs_6_), channel_id=1, source_target_pairs={{0,1},{1,0},{2,3},{3,2},{4,5},{5,4},{6,7},{7,6},{8,9},{9,8},{10,11... | collective-permute-start | bytes 2359304 | tf_op jit(solution)/shard_map/ppermute | solution.py:175
  180.0 0.9 copy-start.7
  180.0 2.3 collective-permute-start.8
  180.8 1.4 copy-start.8
  182.3 0.9 copy-start.9
  200.6 4.9 %copy-start.5 = (f32[256,2]{0,1:T(2,128)S(1)}, f32[256,2]{0,1:T(2,128)}, u32[]{:S(2)}) copy-start(f32[256,2]{0,1:T(2,128)} %param.27) | copy-start | bytes 6148
  200.6 41.8 %all-to-all-start.2 = ((bf16[4,192,2048]{2,1,0:T(8,128)(2,1)}), bf16[4,192,2048]{2,1,0:T(8,128)(2,1)}, u32[]{:S(2)}, u32[]{:S(2)}) async-start(bf16[4,192,2048]{2,1,0:T(8,128)(2,1)} %bitcast.44), calls=%async_computation.2 | async-start | bytes 6291456 | tf_op jit(solution)/shard_map/all_to_all | solution.py:356
Sparse Core Ops, SparseCore 0:
  8.9 99.7 all-gather.2
